TPU v7x, 32 devices: a whole 2x2x4 slice. The times are simulated.
32 devices in a mesh: ep: 16 (over z, y, x), tp: 2 (over core).
Axes of the slice: x: 2, y: 2, z: 4, core: 2. Of those that a mesh axis runs over, the one named last changes fastest.
Arguments:
- tokens: bfloat16 [384, 2048], P('ep'), may hold values from -40 to 40
- old_state: float32 [384, 16, 4096], P('ep', 'tp'), may hold values from -6 to 6
- w_query: bfloat16 [2048, 1024], P(None, 'tp'), may hold values from -0.125 to 0.125
- w_forget: bfloat16 [2048, 1024], P(None, 'tp'), may hold values from -0.125 to 0.125
- w_value: bfloat16 [2048, 1024], P(None, 'tp'), may hold values from -0.125 to 0.125
- w_gate: bfloat16 [2048, 1024], P(None, 'tp'), may hold values from -0.125 to 0.125
- lower_bound: float32 [1024], P('tp'), may hold values from 0.05 to 0.9
- head_gain: float32 [64], replicated, may hold values from 0.1 to 1.9
- w_out: bfloat16 [1024, 2048], P('tp'), may hold values from -0.1875 to 0.1875
- mix_gain: float32 [2048], replicated, may hold values from 0.1 to 1.9
- expert_gate: bfloat16 [16, 2048, 512], P('ep', None, 'tp'), may hold values from -0.125 to 0.125
- expert_up: bfloat16 [16, 2048, 512], P('ep', None, 'tp'), may hold values from -0.125 to 0.125
- expert_down: bfloat16 [16, 512, 2048], P('ep', 'tp'), may hold values from -0.25 to 0.25
- expert_ids: int32 [384, 2], P('ep'), may hold values from 0 to 15, as said below
- route_weight: float32 [384, 2], P('ep'), may hold values from 0.1 to 1
- moe_gain: float32 [2048], replicated, may hold values from 0.1 to 1.9
Outputs:
- next_tokens: bfloat16 [384, 2048], P('ep', 'tp')
- new_state: float32 [384, 16, 4096], P('ep', 'tp')
Inputs may be any that keep to these rules, and one draw needn't show every extreme that they name: `expert_ids`: each row names two different experts of one group of 4 consecutive experts. In each aligned block of 24 rows no expert is named by more than 6 rows, and one expert, the same in every block, is named by exactly 6 rows of every block.
All inputs are finite; a program needn't handle non-finite values.
Results may differ from a plain program's by a relative error of at most 0.011.
Values may be sent and summed in bfloat16 or wider, within the bound.
A program may use at most 128 MiB of HBM per device.

v0:
```python
import jax
import jax.numpy as jnp
from jax import lax
from jax.sharding import PartitionSpec as P


def layer_normed(values, gain):
    center = jnp.mean(values, -1, keepdims=True)
    centered = values - center
    variance = jnp.mean(centered * centered, -1, keepdims=True)
    return centered * lax.rsqrt(variance + 1e-05) * gain


def rounded(values):
    return lax.optimization_barrier(values.astype(jnp.bfloat16)).astype(jnp.float32)


def slot_table(ids_block, expert_count, capacity):
    flat_ids = ids_block.reshape(-1)
    onehot = (flat_ids[:, None] == jnp.arange(expert_count, dtype=jnp.int32)[None, :]).astype(
        jnp.int32
    )
    before = jnp.cumsum(onehot, 0) - onehot
    rank = jnp.sum(before * onehot, 1)
    return flat_ids * capacity + rank


def per_device(
    tokens,
    old_state,
    w_query,
    w_forget,
    w_value,
    w_gate,
    lower_bound,
    head_gain,
    w_out,
    mix_gain,
    expert_gate,
    expert_up,
    expert_down,
    expert_ids,
    route_weight,
    moe_gain,
):
    row_count, model_width = tokens.shape
    heads_here = old_state.shape[1]
    head_dim = head_gain.shape[0]
    head_cols = w_query.shape[1]
    q_lin = jnp.dot(tokens, w_query, preferred_element_type=jnp.float32)
    f_lin = jnp.dot(tokens, w_forget, preferred_element_type=jnp.float32)
    v_lin = jnp.dot(tokens, w_value, preferred_element_type=jnp.float32)
    g_lin = jnp.dot(tokens, w_gate, preferred_element_type=jnp.float32)
    act_query = jax.nn.silu(q_lin).reshape(row_count, heads_here, head_dim)
    bound = lower_bound.reshape(heads_here, head_dim)
    forget = bound + (1.0 - bound) * jax.nn.sigmoid(f_lin.reshape(row_count, heads_here, head_dim))
    previous = old_state.reshape(row_count, heads_here, head_dim, head_dim)
    new_state = forget[..., None] * previous + (1.0 - forget)[..., None] * v_lin.reshape(
        row_count, heads_here, 1, head_dim
    )
    readout = jnp.einsum("shi,shij->shj", act_query, new_state, precision=lax.Precision.HIGHEST)
    normed = readout * lax.rsqrt(jnp.mean(readout * readout, -1, keepdims=True) + 1e-06) * head_gain
    mixer_out = (
        (normed * jax.nn.silu(g_lin.reshape(row_count, heads_here, head_dim)))
        .reshape(row_count, head_cols)
        .astype(jnp.bfloat16)
    )
    own_part = rounded(jnp.dot(mixer_out, w_out, preferred_element_type=jnp.float32))
    mixed = lax.psum(own_part.astype(jnp.bfloat16), "tp").astype(jnp.float32)
    after_mixer = layer_normed(tokens.astype(jnp.float32) + mixed, mix_gain).astype(jnp.bfloat16)
    expert_count = lax.axis_size("ep")
    core_count = lax.axis_size("tp")
    top_count = expert_ids.shape[1]
    capacity = max(2, 2 * top_count * row_count // expert_count)
    slot_ids = slot_table(expert_ids, expert_count, capacity)
    choose = (
        slot_ids[None, :] == jnp.arange(expert_count * capacity, dtype=jnp.int32)[:, None]
    ).astype(jnp.bfloat16)
    choose = choose.reshape(expert_count * capacity, row_count, top_count).sum(-1)
    outgoing = jnp.dot(choose, after_mixer, preferred_element_type=jnp.float32).astype(jnp.bfloat16)
    outgoing = outgoing.reshape(expert_count, capacity, model_width)
    arrived = lax.all_to_all(outgoing, "ep", split_axis=0, concat_axis=0, tiled=True)
    sources = arrived.shape[0]
    slots_now = arrived.shape[1]
    rows_in = arrived.reshape(sources * slots_now, model_width)
    gate_act = jnp.dot(rows_in, expert_gate[0], preferred_element_type=jnp.float32)
    up_act = jnp.dot(rows_in, expert_up[0], preferred_element_type=jnp.float32)
    hidden = (jax.nn.silu(gate_act) * up_act).astype(jnp.bfloat16)
    partial_rows = rounded(jnp.dot(hidden, expert_down[0], preferred_element_type=jnp.float32))
    summed_rows = lax.psum_scatter(
        partial_rows.astype(jnp.bfloat16), "tp", scatter_dimension=1, tiled=True
    ).astype(jnp.float32)
    results = summed_rows.astype(jnp.bfloat16).reshape(sources, slots_now, summed_rows.shape[1])
    back_half = lax.all_to_all(results, "ep", split_axis=0, concat_axis=0, tiled=True)
    returned = lax.all_gather(back_half, "tp", axis=2, tiled=True)
    flat_back = returned.reshape(expert_count * capacity, model_width)
    picked = (
        jnp.take(flat_back, slot_ids, axis=0)
        .reshape(row_count, top_count, model_width)
        .astype(jnp.float32)
    )
    moe_sum = jnp.sum(picked * route_weight[..., None], 1)
    full_rows = layer_normed(after_mixer.astype(jnp.float32) + moe_sum, moe_gain).astype(
        jnp.bfloat16
    )
    half_width = model_width // core_count
    next_tokens = lax.dynamic_slice_in_dim(
        full_rows, lax.axis_index("tp") * half_width, half_width, 1
    )
    return (next_tokens, new_state.reshape(row_count, heads_here, head_dim * head_dim))


def solution(mesh):
    in_specs = (
        P("ep", None),
        P("ep", "tp", None),
        P(None, "tp"),
        P(None, "tp"),
        P(None, "tp"),
        P(None, "tp"),
        P("tp"),
        P(),
        P("tp", None),
        P(),
        P("ep", None, "tp"),
        P("ep", None, "tp"),
        P("ep", "tp", None),
        P("ep", None),
        P("ep", None),
        P(),
    )
    out_specs = (P("ep", "tp"), P("ep", "tp", None))
    return jax.shard_map(
        per_device, mesh=mesh, in_specs=in_specs, out_specs=out_specs, check_vma=False
    )
```

profile of v0, /device:TPU:0, one launch (start us, length us, event | category | flops | bytes accessed | tf_op | source)
XLA Modules:
  0.0 128.8 jit_solution(17914694816942390285)
XLA Ops:
  7.2 0.9 add.128
  8.1 2.1 %fusion.7 = f32[24,512]{1,0:T(8,128)S(1)} fusion(bf16[24,2048]{1,0:T(8,128)(2,1)} %param.16, bf16[2048,512]{1,0:T(8,128)(2,1)} %param.19), kind=kOutput, calls=%fused_computation.15 | convolution fusion | flops 50368512 | bytes 2244608 | tf_op jit(solution)/shard_map/dot_general | solution.py:51
  10.3 2.0 %fusion.33 = f32[24,512]{1,0:T(8,128)S(1)} fusion(bf16[24,2048]{1,0:T(8,128)(2,1)} %param.16, bf16[2048,512]{1,0:T(8,128)(2,1)} %param.20), kind=kOutput, calls=%fused_computation.66 | convolution fusion | flops 50331648 | bytes 2244608 | tf_op jit(solution)/shard_map/dot_general | solution.py:52
  12.4 6.1 %reshape.162 = f32[24,8,64,64]{3,2,1,0:T(8,128)} reshape(f32[24,8,4096]{2,1,0:T(8,128)} %param.17) | data formatting | bytes 6291456 | tf_op jit(solution)/shard_map/reshape | solution.py:57
  18.5 2.0 %divide_multiply_fusion = f32[24,512]{1,0:T(8,128)S(1)} fusion(bf16[24,2048]{1,0:T(8,128)(2,1)S(1)} %copy-done.1, bf16[2048,512]{1,0:T(8,128)(2,1)} %param.18), kind=kOutput, calls=%fused_computation.44 | convolution fusion | flops 50380800 | bytes 2244608 | tf_op jit(solution)/shard_map/dot_general | solution.py:50
  20.7 9.6 %fusion = f32[24,8,1,64]{3,2,1,0:T(1,128)S(1)} fusion(f32[24,8,64,1]{2,3,1,0:T(1,128)S(1)} %bitcast.40, f32[24,8,64,64]{3,2,1,0:T(8,128)} %reshape.162, f32[24,8,64]{2,1,0:T(8,128)S(1)} %get-tuple-element.7, f32[24,8,64]{2,1,0:T(8,128)S(1)} %mul.165, f32[24,8,64]{2,1,0:T(8,128)S(1)} %get-tuple-element.6), kind=kOutput, calls=%fused_computation.1 | convolution fusion | flops 11796480 | bytes 3391488 | tf_op jit(solution)/shard_map/shi,shij->shj/dot_general | solution.py:61
  30.4 0.4 fusion.34
  31.1 1.0 convolution_convert_fusion.2
  32.6 0.2 select_reduce_fusion
  33.0 19.9 %all-reduce.2.cloned.1.call-done = bf16[24,2048]{1,0:T(8,128)(2,1)} async-done(((bf16[24,2048]{1,0:T(8,128)(2,1)}), bf16[24,2048]{1,0:T(8,128)(2,1)}) %all-reduce.2.cloned.1.call-update) | async-done | bytes 98320 | tf_op jit(solution)/shard_map/psum | solution.py:69
  52.9 1.0 fusion.14
  53.9 1.1 multiply_reduce_fusion.2
  55.1 1.0 multiply_convert_fusion
  56.1 0.3 convolution_convert_fusion.1
  56.4 0.9 reshape.165
  57.3 6.8 %all-to-all-start = ((bf16[16,6,2048]{2,1,0:T(8,128)(2,1)}), bf16[16,6,2048]{2,1,0:T(8,128)(2,1)S(1)}, u32[]{:S(2)}, u32[]{:S(2)}) async-start(bf16[16,6,2048]{2,1,0:T(8,128)(2,1)} %reshape.165), calls=%async_computation | async-start | bytes 1048576 | tf_op jit(solution)/shard_map/all_to_all | solution.py:82
  64.2 3.8 %broadcast_multiply_fusion = f32[24,8,64,64]{3,2,1,0:T(8,128)} fusion(f32[24,8,64]{2,1,0:T(8,128)S(1)} %mul.165, f32[24,8,64]{2,1,0:T(8,128)S(1)} %get-tuple-element.6), kind=kLoop, calls=%fused_computation.5 | loop fusion | flops 786432 | bytes 3244032 | tf_op jit(solution)/shard_map/mul | solution.py:58
  68.0 5.8 %mul.196 = f32[24,8,4096]{2,1,0:T(8,128)} reshape(f32[24,8,64,64]{3,2,1,0:T(8,128)} %broadcast_multiply_fusion) | data formatting | bytes 6291456 | tf_op jit(solution)/shard_map/mul | solution.py:58
  73.8 3.8 %mul.162 = f32[24,8,64,64]{3,2,1,0:T(8,128)} broadcast(f32[24,8,64]{2,1,0:T(8,128)S(1)} %get-tuple-element.7), dimensions={0,1,2} | broadcast | bytes 3194880 | tf_op jit(solution)/shard_map/mul | solution.py:58
  77.6 5.9 %mul.194 = f32[24,8,4096]{2,1,0:T(8,128)} reshape(f32[24,8,64,64]{3,2,1,0:T(8,128)} %mul.162) | data formatting | bytes 6291456 | tf_op jit(solution)/shard_map/mul | solution.py:58
  83.7 1.5 %fusion.11 = f32[96,256]{1,0:T(8,128)S(1)} fusion(bf16[96,2048]{1,0:T(8,128)(2,1)S(1)} %reshape.166, bf16[1,2048,256]{2,1,0:T(8,128)(2,1)} %param.26), kind=kOutput, calls=%fused_computation.18 | convolution fusion | flops 100663296 | bytes 1540096 | tf_op jit(solution)/shard_map/dot_general | solution.py:86
  85.2 3.1 %convolution_convert_fusion = bf16[96,2048]{1,0:T(8,128)(2,1)} fusion(bf16[96,2048]{1,0:T(8,128)(2,1)S(1)} %reshape.166, bf16[1,256,2048]{2,1,0:T(8,128)(2,1)} %param.28, bf16[1,2048,256]{2,1,0:T(8,128)(2,1)} %param.27, f32[96,256]{1,0:T(8,128)S(1)} %fusion.11), kind=kOutput, calls=%fused_computation.7 | convolution fusion | flops 201670656 | bytes 2981888 | tf_op jit(solution)/shard_map/dot_general | solution.py:89
  88.3 6.2 %multiply_add_fusion = f32[24,8,4096]{2,1,0:T(8,128)} fusion(f32[24,8,4096]{2,1,0:T(8,128)} %mul.196, f32[24,8,4096]{2,1,0:T(8,128)} %mul.194, f32[24,8,4096]{2,1,0:T(8,128)} %param.17), kind=kLoop, calls=%fused_computation.4 | loop fusion | flops 1572864 | bytes 12582912 | tf_op jit(solution)/shard_map/add | solution.py:58
  94.5 3.1 %reduce-scatter.2.cloned.1.call-done = bf16[96,1024]{1,0:T(8,128)(2,1)} async-done(((bf16[96,2048]{1,0:T(8,128)(2,1)}), bf16[96,1024]{1,0:T(8,128)(2,1)}) %reduce-scatter.2.cloned.1.call-update) | async-done | bytes 196624 | tf_op jit(solution)/shard_map/reduce_scatter | solution.py:90
  97.5 1.7 %reshape.167 = bf16[16,6,1024]{2,1,0:T(8,128)(2,1)} reshape(bf16[96,1024]{1,0:T(8,128)(2,1)} %reduce-scatter.2.cloned.1.call-done) | data formatting | bytes 393216 | tf_op jit(solution)/shard_map/reshape | solution.py:93
  99.2 6.7 %all-to-all-start.1 = ((bf16[16,6,1024]{2,1,0:T(8,128)(2,1)}), bf16[16,6,1024]{2,1,0:T(8,128)(2,1)S(1)}, u32[]{:S(2)}, u32[]{:S(2)}) async-start(bf16[16,6,1024]{2,1,0:T(8,128)(2,1)} %reshape.167), calls=%async_computation.2 | async-start | bytes 524288 | tf_op jit(solution)/shard_map/all_to_all | solution.py:94
  106.4 10.0 %all-to-all-done.1 = bf16[16,6,1024]{2,1,0:T(8,128)(2,1)S(1)} async-done(((bf16[16,6,1024]{2,1,0:T(8,128)(2,1)}), bf16[16,6,1024]{2,1,0:T(8,128)(2,1)S(1)}, u32[]{:S(2)}, u32[]{:S(2)}) %all-to-all-start.1) | async-done | bytes 196640 | tf_op jit(solution)/shard_map/all_to_all | solution.py:94
  116.4 2.2 %all_gather.3 = bf16[16,6,2048]{2,1,0:T(8,128)(2,1)S(1)} all-gather(bf16[16,6,1024]{2,1,0:T(8,128)(2,1)S(1)} %all-to-all-done.1), channel_id=1, replica_groups=mesh['ep'=16,'tp'=2] {'tp'}, dimensions={2}, use_global_device_ids=true | all-gather | bytes 589824 | tf_op jit(solution)/shard_map/all_gather | solution.py:95
  118.7 0.7 gather_fusion
  119.5 1.4 %multiply_reduce_fusion = f32[24,2048]{1,0:T(8,128)S(1)} fusion(bf16[24,2,2048]{2,1,0:T(2,128)(2,1)S(1)} %gather.7, pred[24,2]{1,0:T(8,128)(4,1)S(1)} %copy.30, f32[24,2]{1,0:T(8,128)S(1)} %copy.32), kind=kLoop, calls=%fused_computation.20 | loop fusion | flops 344064 | bytes 393456 | tf_op jit(solution)/shard_map/reduce_sum | solution.py:102
  121.0 0.2 multiply_reduce_fusion.1
  121.3 0.7 fusion.18
  (54 shorter events, 2.4 us)
Async XLA Ops:
  7.2 24.0 %copy-start = (bf16[512,2048]{1,0:T(8,128)(2,1)S(1)}, bf16[512,2048]{1,0:T(8,128)(2,1)}, u32[]{:S(2)}) copy-start(bf16[512,2048]{1,0:T(8,128)(2,1)} %param.24) | copy-start | bytes 6291460
  7.2 45.7 %all-reduce.2.cloned.1.call-start = ((), (), s32[]{:S(2)}) async-start(), calls=%async_computation.3 | async-start | bytes 196608 | tf_op jit(solution)/shard_map/psum | solution.py:69
  12.4 6.1 %copy-start.1 = (bf16[24,2048]{1,0:T(8,128)(2,1)S(1)}, bf16[24,2048]{1,0:T(8,128)(2,1)}, u32[]{:S(2)}) copy-start(bf16[24,2048]{1,0:T(8,128)(2,1)} %param.16) | copy-start | bytes 294916
  20.6 9.8 %copy-start.2 = (bf16[2048,512]{1,0:T(8,128)(2,1)S(1)}, bf16[2048,512]{1,0:T(8,128)(2,1)}, u32[]{:S(2)}) copy-start(bf16[2048,512]{1,0:T(8,128)(2,1)} %param.21) | copy-start | bytes 6291460
  20.7 10.3 %copy-start.6 = (f32[64]{0:T(128)S(1)}, f32[64]{0:T(128)}, u32[]{:S(2)}) copy-start(f32[64]{0:T(128)} %param.23) | copy-start | bytes 772
  30.3 1.9 %copy-start.3 = (s32[24,2]{0,1:T(2,128)S(1)}, s32[24,2]{0,1:T(2,128)}, u32[]{:S(2)}) copy-start(s32[24,2]{0,1:T(2,128)} %param.29) | copy-start | bytes 580
  30.3 24.8 %copy-start.4 = (f32[2048]{0:T(1024)S(1)}, f32[2048]{0:T(1024)}, u32[]{:S(2)}) copy-start(f32[2048]{0:T(1024)} %param.25) | copy-start | bytes 24580
  57.3 26.2 %all-to-all-start = ((bf16[16,6,2048]{2,1,0:T(8,128)(2,1)}), bf16[16,6,2048]{2,1,0:T(8,128)(2,1)S(1)}, u32[]{:S(2)}, u32[]{:S(2)}) async-start(bf16[16,6,2048]{2,1,0:T(8,128)(2,1)} %reshape.165), calls=%async_computation | async-start | bytes 1048576 | tf_op jit(solution)/shard_map/all_to_all | solution.py:82
  64.1 33.4 %reduce-scatter.2.cloned.1.call-start = ((), (), s32[]{:S(2)}) async-start(), calls=%async_computation.4 | async-start | bytes 589824 | tf_op jit(solution)/shard_map/reduce_scatter | solution.py:90
  88.3 18.0 %copy-start.5 = (f32[24,2]{0,1:T(2,128)S(1)}, f32[24,2]{0,1:T(2,128)}, u32[]{:S(2)}) copy-start(f32[24,2]{0,1:T(2,128)} %param.30) | copy-start | bytes 580
  99.2 17.1 %all-to-all-start.1 = ((bf16[16,6,1024]{2,1,0:T(8,128)(2,1)}), bf16[16,6,1024]{2,1,0:T(8,128)(2,1)S(1)}, u32[]{:S(2)}, u32[]{:S(2)}) async-start(bf16[16,6,1024]{2,1,0:T(8,128)(2,1)} %reshape.167), calls=%async_computation.2 | async-start | bytes 524288 | tf_op jit(solution)/shard_map/all_to_all | solution.py:94
  106.3 14.9 %dynamic-slice-start = ((f32[2048]{0:T(1024)}, s32[]{:T(128)}), f32[1024]{0:T(1024)S(1)}, s32[]{:S(2)}) async-start(f32[2048]{0:T(1024)} %param.31, s32[]{:T(128)} %select_n.28), calls=%async_computation.5 | async-start | bytes 8704 | tf_op jit(solution)/shard_map/dynamic_slice | solution.py:107
Sparse Core Ops, SparseCore 0:
  32.3 20.5 all-reduce.1
  88.4 9.0 reduce-scatter.1
where the time goes:
time: 130 us; the launch traced here: 129 us
  waiting for transfers between devices  33 us (25%)
  local copies, waits for them, and re-layouts  27.5 us (21%)
  matrix products  22 us (17%)
  other arithmetic  16.2 us (12%)
  between operations  14.3 us (11%)
  starting transfers between devices  13.6 us (10%)
  blocking collectives  2.17 us (2%)
    psum x1, waiting for transfers between devices, per_device(): mixed = lax.psum(own_part.astype(jnp.bfloat16), 'tp').astype(jnp.float32)  19.9 us
    all_to_all x1, waiting for transfers between devices, per_device(): lax.all_to_all(results, 'ep', split_axis=0, concat_axis=0, tiled=True)  9.99 us
    mul x2, local copies, waits for them, and re-layouts, per_device(): forget[..., None] * previous  9.72 us
    dot_general x1, matrix products, per_device(): jnp.einsum('shi,shij->shj', act_query, new_state, precision=lax.Precision...  9.61 us
    all_to_all x1, starting transfers between devices, per_device(): lax.all_to_all(outgoing, 'ep', split_axis=0, concat_axis=0, tiled=True)  6.82 us
    all_to_all x1, starting transfers between devices, per_device(): lax.all_to_all(results, 'ep', split_axis=0, concat_axis=0, tiled=True)  6.74 us
    add x1, other arithmetic, per_device(): forget[..., None] * previous  6.17 us
    reshape x1, local copies, waits for them, and re-layouts, per_device(): previous = old_state.reshape(row_count, heads_here, head_dim, head_dim)  6.14 us
  transfers between devices with their start and end apart: 4, of which 3 were waited for; matrix products, arithmetic and copies ran while one was open for 21% of the time, Pallas kernels for 0%

commit v1 on v0

--- a/solution.py
+++ b/solution.py
@@ -66,7 +66,7 @@
         .astype(jnp.bfloat16)
     )
     own_part = rounded(jnp.dot(mixer_out, w_out, preferred_element_type=jnp.float32))
-    mixed = lax.psum(own_part.astype(jnp.bfloat16), "tp").astype(jnp.float32)
+    mixed = jnp.sum(lax.all_gather(own_part.astype(jnp.bfloat16), "tp"), axis=0).astype(jnp.float32)
     after_mixer = layer_normed(tokens.astype(jnp.float32) + mixed, mix_gain).astype(jnp.bfloat16)
     expert_count = lax.axis_size("ep")
     core_count = lax.axis_size("tp")

time: 130 us -> 110 us (0.85)
  waiting for transfers between devices: 33 us -> 13.1 us
  other arithmetic: 16.2 us -> 13.6 us
  blocking collectives: 2.17 us -> 4.25 us
  starting transfers between devices: 13.6 us -> 15 us
    psum x1 -> x0, waiting for transfers between devices: 19.9 us -> none  [per_device(): mixed = lax.psum(own_part.astype(jnp.bfloat16), 'tp').astype(jnp.float32)]
    all_gather x0 -> x1, blocking collectives: none -> 2.08 us  [per_device(): lax.all_gather(own_part.astype(jnp.bfloat16), 'tp')]
    all_to_all x1, starting transfers between devices: 6.82 us -> 8.21 us  [per_device(): lax.all_to_all(outgoing, 'ep', split_axis=0, concat_axis=0, tiled=True)]
  transfers between devices with their start and end apart: 4 -> 3, of which waited for: 3 -> 2; matrix products, arithmetic and copies ran while one was open for 21% -> 24% of each run, Pallas kernels for 0% -> 0%
where the time goes in v1:
time: 110 us; the launch traced here: 109 us
  local copies, waits for them, and re-layouts  27.5 us (25%)
  matrix products  21.3 us (19%)
  starting transfers between devices  15 us (14%)
  between operations  14.3 us (13%)
  other arithmetic  13.6 us (12%)
  waiting for transfers between devices  13.1 us (12%)
  blocking collectives  4.25 us (4%)
    all_to_all x1, waiting for transfers between devices, per_device(): lax.all_to_all(results, 'ep', split_axis=0, concat_axis=0, tiled=True)  9.97 us
    mul x2, local copies, waits for them, and re-layouts, per_device(): forget[..., None] * previous  9.72 us
    dot_general x1, matrix products, per_device(): jnp.einsum('shi,shij->shj', act_query, new_state, precision=lax.Precision...  9.61 us
    all_to_all x1, starting transfers between devices, per_device(): lax.all_to_all(outgoing, 'ep', split_axis=0, concat_axis=0, tiled=True)  8.21 us
    all_to_all x1, starting transfers between devices, per_device(): lax.all_to_all(results, 'ep', split_axis=0, concat_axis=0, tiled=True)  6.74 us
    add x1, other arithmetic, per_device(): forget[..., None] * previous  6.17 us
    reshape x1, local copies, waits for them, and re-layouts, per_device(): previous = old_state.reshape(row_count, heads_here, head_dim, head_dim)  6.14 us
    mul x2, local copies, waits for them, and re-layouts, per_device(): (1.0 - forget)[..., None]  5.92 us
  transfers between devices with their start and end apart: 3, of which 2 were waited for; matrix products, arithmetic and copies ran while one was open for 24% of the time, Pallas kernels for 0%

profile of v1, /device:TPU:0, one launch (start us, length us, event | category | flops | bytes accessed | tf_op | source)
XLA Modules:
  0.0 109.0 jit_solution(15690993807426451860)
XLA Ops:
  7.2 0.9 add.126
  8.1 2.1 %fusion.7 = f32[24,512]{1,0:T(8,128)S(1)} fusion(bf16[24,2048]{1,0:T(8,128)(2,1)} %param.16, bf16[2048,512]{1,0:T(8,128)(2,1)} %param.19), kind=kOutput, calls=%fused_computation.15 | convolution fusion | flops 50368512 | bytes 2244608 | tf_op jit(solution)/shard_map/dot_general | solution.py:51
  10.2 2.0 %fusion.33 = f32[24,512]{1,0:T(8,128)S(1)} fusion(bf16[24,2048]{1,0:T(8,128)(2,1)} %param.16, bf16[2048,512]{1,0:T(8,128)(2,1)} %param.20), kind=kOutput, calls=%fused_computation.66 | convolution fusion | flops 50331648 | bytes 2244608 | tf_op jit(solution)/shard_map/dot_general | solution.py:52
  12.4 6.1 %reshape.162 = f32[24,8,64,64]{3,2,1,0:T(8,128)} reshape(f32[24,8,4096]{2,1,0:T(8,128)} %param.17) | data formatting | bytes 6291456 | tf_op jit(solution)/shard_map/reshape | solution.py:57
  18.5 2.0 %divide_multiply_fusion = f32[24,512]{1,0:T(8,128)S(1)} fusion(bf16[24,2048]{1,0:T(8,128)(2,1)S(1)} %copy-done.1, bf16[2048,512]{1,0:T(8,128)(2,1)} %param.18), kind=kOutput, calls=%fused_computation.44 | convolution fusion | flops 50380800 | bytes 2244608 | tf_op jit(solution)/shard_map/dot_general | solution.py:50
  20.6 9.6 %fusion = f32[24,8,1,64]{3,2,1,0:T(1,128)S(1)} fusion(f32[24,8,64,1]{2,3,1,0:T(1,128)S(1)} %bitcast.42, f32[24,8,64,64]{3,2,1,0:T(8,128)} %reshape.162, f32[24,8,64]{2,1,0:T(8,128)S(1)} %get-tuple-element.7, f32[24,8,64]{2,1,0:T(8,128)S(1)} %mul.165, f32[24,8,64]{2,1,0:T(8,128)S(1)} %get-tuple-element.6), kind=kOutput, calls=%fused_computation.1 | convolution fusion | flops 11796480 | bytes 3391488 | tf_op jit(solution)/shard_map/shi,shij->shj/dot_general | solution.py:61
  30.4 0.4 fusion.34
  31.1 0.4 convolution_convert_fusion.2
  31.5 2.1 %all-gather = bf16[48,2048]{1,0:T(8,128)(2,1)S(1)} all-gather(bf16[24,2048]{1,0:T(8,128)(2,1)S(1)} %convolution_convert_fusion.2), channel_id=2, replica_groups=mesh['ep'=16,'tp'=2] {'tp'}, dimensions={0}, use_global_device_ids=true | all-gather | bytes 294912 | tf_op jit(solution)/shard_map/all_gather | solution.py:69
  33.6 0.1 fusion.14
  33.8 0.2 multiply_reduce_fusion.2
  34.3 0.2 select_reduce_fusion
  34.9 0.3 convolution_convert_fusion.1
  35.2 0.9 reshape.165
  36.1 8.2 %all-to-all-start = ((bf16[16,6,2048]{2,1,0:T(8,128)(2,1)}), bf16[16,6,2048]{2,1,0:T(8,128)(2,1)S(1)}, u32[]{:S(2)}, u32[]{:S(2)}) async-start(bf16[16,6,2048]{2,1,0:T(8,128)(2,1)} %reshape.165), calls=%async_computation | async-start | bytes 1048576 | tf_op jit(solution)/shard_map/all_to_all | solution.py:82
  44.4 3.8 %broadcast_multiply_fusion = f32[24,8,64,64]{3,2,1,0:T(8,128)} fusion(f32[24,8,64]{2,1,0:T(8,128)S(1)} %mul.165, f32[24,8,64]{2,1,0:T(8,128)S(1)} %get-tuple-element.6), kind=kLoop, calls=%fused_computation.5 | loop fusion | flops 786432 | bytes 3244032 | tf_op jit(solution)/shard_map/mul | solution.py:58
  48.2 5.8 %mul.196 = f32[24,8,4096]{2,1,0:T(8,128)} reshape(f32[24,8,64,64]{3,2,1,0:T(8,128)} %broadcast_multiply_fusion) | data formatting | bytes 6291456 | tf_op jit(solution)/shard_map/mul | solution.py:58
  54.0 3.8 %mul.162 = f32[24,8,64,64]{3,2,1,0:T(8,128)} broadcast(f32[24,8,64]{2,1,0:T(8,128)S(1)} %get-tuple-element.7), dimensions={0,1,2} | broadcast | bytes 3194880 | tf_op jit(solution)/shard_map/mul | solution.py:58
  57.8 5.9 %mul.194 = f32[24,8,4096]{2,1,0:T(8,128)} reshape(f32[24,8,64,64]{3,2,1,0:T(8,128)} %mul.162) | data formatting | bytes 6291456 | tf_op jit(solution)/shard_map/mul | solution.py:58
  63.9 1.5 %fusion.11 = f32[96,256]{1,0:T(8,128)S(1)} fusion(bf16[96,2048]{1,0:T(8,128)(2,1)S(1)} %reshape.166, bf16[1,2048,256]{2,1,0:T(8,128)(2,1)} %param.26), kind=kOutput, calls=%fused_computation.18 | convolution fusion | flops 100663296 | bytes 1540096 | tf_op jit(solution)/shard_map/dot_general | solution.py:86
  65.4 3.1 %convolution_convert_fusion = bf16[96,2048]{1,0:T(8,128)(2,1)} fusion(bf16[96,2048]{1,0:T(8,128)(2,1)S(1)} %reshape.166, bf16[1,256,2048]{2,1,0:T(8,128)(2,1)} %param.28, bf16[1,2048,256]{2,1,0:T(8,128)(2,1)} %param.27, f32[96,256]{1,0:T(8,128)S(1)} %fusion.11), kind=kOutput, calls=%fused_computation.7 | convolution fusion | flops 201670656 | bytes 2981888 | tf_op jit(solution)/shard_map/dot_general | solution.py:89
  68.5 6.2 %multiply_add_fusion = f32[24,8,4096]{2,1,0:T(8,128)} fusion(f32[24,8,4096]{2,1,0:T(8,128)} %mul.196, f32[24,8,4096]{2,1,0:T(8,128)} %mul.194, f32[24,8,4096]{2,1,0:T(8,128)} %param.17), kind=kLoop, calls=%fused_computation.4 | loop fusion | flops 1572864 | bytes 12582912 | tf_op jit(solution)/shard_map/add | solution.py:58
  74.7 3.1 %reduce-scatter.2.cloned.1.call-done = bf16[96,1024]{1,0:T(8,128)(2,1)} async-done(((bf16[96,2048]{1,0:T(8,128)(2,1)}), bf16[96,1024]{1,0:T(8,128)(2,1)}) %reduce-scatter.2.cloned.1.call-update) | async-done | bytes 196624 | tf_op jit(solution)/shard_map/reduce_scatter | solution.py:90
  77.7 1.7 %reshape.167 = bf16[16,6,1024]{2,1,0:T(8,128)(2,1)} reshape(bf16[96,1024]{1,0:T(8,128)(2,1)} %reduce-scatter.2.cloned.1.call-done) | data formatting | bytes 393216 | tf_op jit(solution)/shard_map/reshape | solution.py:93
  79.4 6.7 %all-to-all-start.1 = ((bf16[16,6,1024]{2,1,0:T(8,128)(2,1)}), bf16[16,6,1024]{2,1,0:T(8,128)(2,1)S(1)}, u32[]{:S(2)}, u32[]{:S(2)}) async-start(bf16[16,6,1024]{2,1,0:T(8,128)(2,1)} %reshape.167), calls=%async_computation.2 | async-start | bytes 524288 | tf_op jit(solution)/shard_map/all_to_all | solution.py:94
  86.6 10.0 %all-to-all-done.1 = bf16[16,6,1024]{2,1,0:T(8,128)(2,1)S(1)} async-done(((bf16[16,6,1024]{2,1,0:T(8,128)(2,1)}), bf16[16,6,1024]{2,1,0:T(8,128)(2,1)S(1)}, u32[]{:S(2)}, u32[]{:S(2)}) %all-to-all-start.1) | async-done | bytes 196640 | tf_op jit(solution)/shard_map/all_to_all | solution.py:94
  96.6 2.2 %all_gather.11 = bf16[16,6,2048]{2,1,0:T(8,128)(2,1)S(1)} all-gather(bf16[16,6,1024]{2,1,0:T(8,128)(2,1)S(1)} %all-to-all-done.1), channel_id=1, replica_groups=mesh['ep'=16,'tp'=2] {'tp'}, dimensions={2}, use_global_device_ids=true | all-gather | bytes 589824 | tf_op jit(solution)/shard_map/all_gather | solution.py:95
  98.9 0.7 gather_fusion
  99.6 0.1 gather.7
  99.7 1.4 %multiply_reduce_fusion = f32[24,2048]{1,0:T(8,128)S(1)} fusion(bf16[24,2,2048]{2,1,0:T(2,128)(2,1)S(1)} %gather.7, pred[24,2]{1,0:T(8,128)(4,1)S(1)} %copy.30, f32[24,2]{1,0:T(8,128)S(1)} %copy.32), kind=kLoop, calls=%fused_computation.20 | loop fusion | flops 344064 | bytes 393456 | tf_op jit(solution)/shard_map/reduce_sum | solution.py:102
  101.3 0.2 multiply_reduce_fusion.1
  101.5 0.7 fusion.18
  (53 shorter events, 2.3 us)
Async XLA Ops:
  7.2 23.9 %copy-start = (bf16[512,2048]{1,0:T(8,128)(2,1)S(1)}, bf16[512,2048]{1,0:T(8,128)(2,1)}, u32[]{:S(2)}) copy-start(bf16[512,2048]{1,0:T(8,128)(2,1)} %param.24) | copy-start | bytes 6291460
  12.4 6.1 %copy-start.1 = (bf16[24,2048]{1,0:T(8,128)(2,1)S(1)}, bf16[24,2048]{1,0:T(8,128)(2,1)}, u32[]{:S(2)}) copy-start(bf16[24,2048]{1,0:T(8,128)(2,1)} %param.16) | copy-start | bytes 294916
  20.6 9.8 %copy-start.2 = (bf16[2048,512]{1,0:T(8,128)(2,1)S(1)}, bf16[2048,512]{1,0:T(8,128)(2,1)}, u32[]{:S(2)}) copy-start(bf16[2048,512]{1,0:T(8,128)(2,1)} %param.21) | copy-start | bytes 6291460
  20.6 10.3 %copy-start.6 = (f32[64]{0:T(128)S(1)}, f32[64]{0:T(128)}, u32[]{:S(2)}) copy-start(f32[64]{0:T(128)} %param.23) | copy-start | bytes 772
  30.3 3.7 %copy-start.3 = (s32[24,2]{0,1:T(2,128)S(1)}, s32[24,2]{0,1:T(2,128)}, u32[]{:S(2)}) copy-start(s32[24,2]{0,1:T(2,128)} %param.29) | copy-start | bytes 580
  30.3 4.5 %copy-start.4 = (f32[2048]{0:T(1024)S(1)}, f32[2048]{0:T(1024)}, u32[]{:S(2)}) copy-start(f32[2048]{0:T(1024)} %param.25) | copy-start | bytes 24580
  36.1 27.6 %all-to-all-start = ((bf16[16,6,2048]{2,1,0:T(8,128)(2,1)}), bf16[16,6,2048]{2,1,0:T(8,128)(2,1)S(1)}, u32[]{:S(2)}, u32[]{:S(2)}) async-start(bf16[16,6,2048]{2,1,0:T(8,128)(2,1)} %reshape.165), calls=%async_computation | async-start | bytes 1048576 | tf_op jit(solution)/shard_map/all_to_all | solution.py:82
  44.3 33.4 %reduce-scatter.2.cloned.1.call-start = ((), (), s32[]{:S(2)}) async-start(), calls=%async_computation.3 | async-start | bytes 589824 | tf_op jit(solution)/shard_map/reduce_scatter | solution.py:90
  68.5 18.0 %copy-start.5 = (f32[24,2]{0,1:T(2,128)S(1)}, f32[24,2]{0,1:T(2,128)}, u32[]{:S(2)}) copy-start(f32[24,2]{0,1:T(2,128)} %param.30) | copy-start | bytes 580
  79.4 17.1 %all-to-all-start.1 = ((bf16[16,6,1024]{2,1,0:T(8,128)(2,1)}), bf16[16,6,1024]{2,1,0:T(8,128)(2,1)S(1)}, u32[]{:S(2)}, u32[]{:S(2)}) async-start(bf16[16,6,1024]{2,1,0:T(8,128)(2,1)} %reshape.167), calls=%async_computation.2 | async-start | bytes 524288 | tf_op jit(solution)/shard_map/all_to_all | solution.py:94
  86.6 14.9 %dynamic-slice-start = ((f32[2048]{0:T(1024)}, s32[]{:T(128)}), f32[1024]{0:T(1024)S(1)}, s32[]{:S(2)}) async-start(f32[2048]{0:T(1024)} %param.31, s32[]{:T(128)} %select_n.28), calls=%async_computation.4 | async-start | bytes 8704 | tf_op jit(solution)/shard_map/dynamic_slice | solution.py:107
Sparse Core Ops, SparseCore 0:
  68.6 9.0 reduce-scatter.1
